TPU v7x, 32 devices: a whole 2x2x4 slice. The times are simulated.
32 devices in a mesh: fs: 8 (over z, y), tp: 4 (over x, core).
Axes of the slice: x: 2, y: 2, z: 4, core: 2. Of those that a mesh axis runs over, the one named last changes fastest.
Arguments:
- h_saved: bfloat16 [4096, 4096], P('fs'), may hold values from -8 to 8
- y_saved: bfloat16 [4096, 2048], P('fs'), may hold values from -8 to 8
- d_gate: bfloat16 [4096, 2048], P('fs', 'tp'), may hold values from -0.25 to 0.25
- d_out: bfloat16 [4096, 4096], P('fs', 'tp'), may hold values from -0.25 to 0.25
- p_gate: bfloat16 [4096, 256], P('fs'), may hold values from -2 to 2
- p_out: bfloat16 [2048, 256], P('fs'), may hold values from -2 to 2
- w_gate: float32 [4096, 2048], P('fs', 'tp'), may hold values from -6 to 6
- w_out: float32 [2048, 4096], P('fs', 'tp'), may hold values from -6 to 6
- m_gate: float32 [256, 2048], P('fs', 'tp'), may hold values from -4 to 4
- m_out: float32 [256, 4096], P('fs', 'tp'), may hold values from -4 to 4
- v_gate: float32 [256, 2048], P('fs', 'tp'), may hold values from 0.02 to 0.2
- v_out: float32 [256, 4096], P('fs', 'tp'), may hold values from 0.02 to 0.2
Outputs:
- step_gate: float32 [4096, 2048], P('fs', 'tp')
- step_out: float32 [2048, 4096], P('fs', 'tp')
- moment_gate: float32 [256, 2048], P('fs', 'tp')
- moment_out: float32 [256, 4096], P('fs', 'tp')
- second_gate: float32 [256, 2048], P('fs', 'tp')
- second_out: float32 [256, 4096], P('fs', 'tp')
- copy_gate: bfloat16 [4096, 2048], P(None, 'tp')
- copy_out: bfloat16 [2048, 4096], P(None, 'tp')
All inputs are finite; a program needn't handle non-finite values.
Results may differ from a plain program's by a relative error of at most 0.001.
Values may be sent and summed in bfloat16 or wider, within the bound.
A program may use at most 64 MiB of HBM per device.

v0:
```python
import jax
import jax.numpy as jnp
from jax import lax
from jax.sharding import PartitionSpec as P

BETA_ONE = 0.9
BETA_TWO = 0.95
LEARN_RATE = 0.1
EPSILON = 1e-06
TOKEN_DIMS = (((0,), (0,)), ((), ()))


def projected_partial(saved, cotangent, factor):
    reduced = jnp.dot(
        saved, lax.all_gather(factor, "fs", axis=0, tiled=True), preferred_element_type=jnp.float32
    )
    return lax.dot_general(
        reduced,
        cotangent.astype(jnp.float32),
        TOKEN_DIMS,
        precision=lax.Precision.HIGHEST,
        preferred_element_type=jnp.float32,
    )


def on_device(
    h_saved, y_saved, d_gate, d_out, p_gate, p_out, w_gate, w_out, m_gate, m_out, v_gate, v_out
):
    part_gate = projected_partial(h_saved, d_gate, p_gate)
    part_out = projected_partial(y_saved, d_out, p_out)
    proj_gate, proj_out = (
        lax.psum_scatter(part_gate, "fs", scatter_dimension=0, tiled=True),
        lax.psum_scatter(part_out, "fs", scatter_dimension=0, tiled=True),
    )
    moment_gate = BETA_ONE * m_gate + (1.0 - BETA_ONE) * proj_gate
    moment_out = BETA_ONE * m_out + (1.0 - BETA_ONE) * proj_out
    second_gate = BETA_TWO * v_gate + (1.0 - BETA_TWO) * proj_gate * proj_gate
    second_out = BETA_TWO * v_out + (1.0 - BETA_TWO) * proj_out * proj_out
    normed_gate = moment_gate / jnp.sqrt(second_gate)
    normed_out = moment_out / jnp.sqrt(second_out)
    whole_gate, whole_out = (
        lax.all_gather(normed_gate, "fs", axis=0, tiled=True),
        lax.all_gather(normed_out, "fs", axis=0, tiled=True),
    )
    update_gate = jnp.dot(p_gate.astype(jnp.float32), whole_gate, precision=lax.Precision.HIGHEST)
    update_out = jnp.dot(p_out.astype(jnp.float32), whole_out, precision=lax.Precision.HIGHEST)
    squares = lax.psum(
        (jnp.sum(update_gate * update_gate), jnp.sum(update_out * update_out)), ("fs", "tp")
    )
    devices_all = lax.axis_size("fs") * lax.axis_size("tp")
    step_gate = update_gate * lax.rsqrt(squares[0] / (update_gate.size * devices_all) + EPSILON)
    step_out = update_out * lax.rsqrt(squares[1] / (update_out.size * devices_all) + EPSILON)
    local_gate = (w_gate - LEARN_RATE * step_gate).astype(jnp.bfloat16)
    local_out = (w_out - LEARN_RATE * step_out).astype(jnp.bfloat16)
    copy_gate, copy_out = (
        lax.all_gather(local_gate, "fs", axis=0, tiled=True),
        lax.all_gather(local_out, "fs", axis=0, tiled=True),
    )
    return (
        step_gate,
        step_out,
        moment_gate,
        moment_out,
        second_gate,
        second_out,
        copy_gate,
        copy_out,
    )


def solution(mesh):
    placed = (
        P("fs", None),
        P("fs", None),
        P("fs", "tp"),
        P("fs", "tp"),
        P("fs", None),
        P("fs", None),
        P("fs", "tp"),
        P("fs", "tp"),
        P("fs", "tp"),
        P("fs", "tp"),
        P("fs", "tp"),
        P("fs", "tp"),
    )
    return jax.shard_map(
        on_device,
        mesh=mesh,
        in_specs=placed,
        out_specs=(
            P("fs", "tp"),
            P("fs", "tp"),
            P("fs", "tp"),
            P("fs", "tp"),
            P("fs", "tp"),
            P("fs", "tp"),
            P(None, "tp"),
            P(None, "tp"),
        ),
        check_vma=False,
    )
```

profile of v0, /device:TPU:0, one launch (start us, length us, event | category | flops | bytes accessed | tf_op | source)
XLA Modules:
  0.0 486.9 jit_solution(17117963242503753305)
XLA Ops:
  8.7 44.4 %all-gather.8.cloned.1.call-done = bf16[2048,256]{1,0:T(8,128)(2,1)} async-done(((bf16[256,256]{1,0:T(8,128)(2,1)}), bf16[2048,256]{1,0:T(8,128)(2,1)}) %all-gather.8.cloned.1.call-update) | async-done | bytes 1048592 | tf_op jit(solution)/shard_map/all_gather | solution.py:15
  53.2 1.9 fusion.6
  55.1 2.0 fusion.7
  57.2 45.9 %all-gather.6.cloned.1.call-done = bf16[4096,256]{1,0:T(8,128)(2,1)} async-done(((bf16[512,256]{1,0:T(8,128)(2,1)}), bf16[4096,256]{1,0:T(8,128)(2,1)}) %all-gather.6.cloned.1.call-update) | async-done | bytes 2097168 | tf_op jit(solution)/shard_map/all_gather | solution.py:15
  103.1 4.2 fusion.4
  107.3 1.4 fusion.5
  108.8 61.0 %reduce-scatter.5.cloned.1.call-done = f32[32,1024]{1,0:T(8,128)} async-done(((f32[256,1024]{1,0:T(8,128)}), f32[32,1024]{1,0:T(8,128)}) %reduce-scatter.5.cloned.1.call-update) | async-done | bytes 131088 | tf_op jit(solution)/shard_map/reduce_scatter | solution.py:33
  169.8 1.8 rsqrt_multiply_fusion
  173.0 62.3 %reduce-scatter.3.cloned.1.call-done = f32[32,512]{1,0:T(8,128)} async-done(((f32[256,512]{1,0:T(8,128)}), f32[32,512]{1,0:T(8,128)}) %reduce-scatter.3.cloned.1.call-update) | async-done | bytes 65552 | tf_op jit(solution)/shard_map/reduce_scatter | solution.py:32
  235.3 1.6 rsqrt_multiply_fusion.1
  236.9 31.7 %all_gather.19 = f32[256,512]{1,0:T(8,128)S(1)} all-gather(f32[32,512]{1,0:T(8,128)S(1)} %get-tuple-element.25), channel_id=1, replica_groups=mesh['fs'=8,'tp'=4] {'fs'}, dimensions={0}, use_global_device_ids=true | all-gather | bytes 589824 | tf_op jit(solution)/shard_map/all_gather | solution.py:42
  268.6 2.6 multiply_reduce_fusion.1
  271.1 7.3 %all-gather.10.cloned.1.call-done = f32[256,1024]{1,0:T(8,128)} async-done(((f32[32,1024]{1,0:T(8,128)}), f32[256,1024]{1,0:T(8,128)}) %all-gather.10.cloned.1.call-update) | async-done | bytes 1048592 | tf_op jit(solution)/shard_map/all_gather | solution.py:43
  278.4 2.8 multiply_reduce_fusion
  281.2 38.7 %all-reduce = (f32[]{:T(128)}, f32[]{:T(128)}) all-reduce(f32[]{:T(128)} %get-tuple-element.28, f32[]{:T(128)} %get-tuple-element.30), channel_id=1, replica_groups=mesh['fs'=8,'tp'=4] {'fs','tp'}, use_global_device_ids=true, to_apply=%region_2.0 | all-reduce | flops 2 | bytes 16 | tf_op jit(solution)/shard_map/psum | solution.py:47
  320.6 2.9 subtract_convert_fusion.1
  323.7 2.5 copy.21
  326.9 2.6 subtract_convert_fusion
  329.5 2.5 copy.22
  332.0 2.6 copy.23
  334.6 64.3 %all-gather.12.cloned.1.call-done = bf16[4096,512]{0,1:T(8,128)(2,1)} async-done(((bf16[512,512]{0,1:T(8,128)(2,1)}), bf16[4096,512]{0,1:T(8,128)(2,1)}) %all-gather.12.cloned.1.call-update) | async-done | bytes 4194320 | tf_op jit(solution)/shard_map/all_gather | solution.py:56
  398.8 6.4 %copy.24 = bf16[4096,512]{1,0:T(8,128)(2,1)} copy(bf16[4096,512]{0,1:T(8,128)(2,1)} %all-gather.12.cloned.1.call-done) | data formatting | bytes 8388608
  405.2 68.5 %all-gather.14.cloned.1.call-done = bf16[2048,1024]{0,1:T(8,128)(2,1)} async-done(((bf16[256,1024]{0,1:T(8,128)(2,1)}), bf16[2048,1024]{0,1:T(8,128)(2,1)}) %all-gather.14.cloned.1.call-update) | async-done | bytes 4194320 | tf_op jit(solution)/shard_map/all_gather | solution.py:57
  473.7 6.4 %copy.25 = bf16[2048,1024]{1,0:T(8,128)(2,1)} copy(bf16[2048,1024]{0,1:T(8,128)(2,1)} %all-gather.14.cloned.1.call-done) | data formatting | bytes 8388608
  (27 shorter events, 3.1 us)
Async XLA Ops:
  7.2 46.0 %copy-start = (bf16[512,2048]{1,0:T(8,128)(2,1)S(1)}, bf16[512,2048]{1,0:T(8,128)(2,1)}, u32[]{:S(2)}) copy-start(bf16[512,2048]{1,0:T(8,128)(2,1)} %param.13) | copy-start | bytes 6291460
  7.2 47.9 %copy-start.1 = (bf16[512,1024]{1,0:T(8,128)(2,1)S(1)}, bf16[512,1024]{1,0:T(8,128)(2,1)}, u32[]{:S(2)}) copy-start(bf16[512,1024]{1,0:T(8,128)(2,1)} %param.15) | copy-start | bytes 3145732
  7.2 46.0 %all-gather.8.cloned.1.call-start = ((), (), s32[]{:S(2)}) async-start(), calls=%async_computation.4 | async-start | bytes 1179648 | tf_op jit(solution)/shard_map/all_gather | solution.py:15
  7.9 95.2 %all-gather.6.cloned.1.call-start = ((), (), s32[]{:S(2)}) async-start(), calls=%async_computation.2 | async-start | bytes 2359296 | tf_op jit(solution)/shard_map/all_gather | solution.py:15
  8.7 161.1 %reduce-scatter.5.cloned.1.call-start = ((), (), s32[]{:S(2)}) async-start(), calls=%async_computation.5 | async-start | bytes 1179648 | tf_op jit(solution)/shard_map/reduce_scatter | solution.py:33
  57.1 114.5 %copy-start.2 = (f32[512,512]{1,0:T(8,128)S(1)}, f32[512,512]{1,0:T(8,128)}, u32[]{:S(2)}) copy-start(f32[512,512]{1,0:T(8,128)} %param.18) | copy-start | bytes 3145732
  57.2 178.1 %reduce-scatter.3.cloned.1.call-start = ((), (), s32[]{:S(2)}) async-start(), calls=%async_computation.3 | async-start | bytes 589824 | tf_op jit(solution)/shard_map/reduce_scatter | solution.py:32
  103.1 4.2 copy-start.4
  107.3 161.3 %copy-start.3 = (bf16[512,256]{1,0:T(8,128)(2,1)S(1)}, bf16[512,256]{1,0:T(8,128)(2,1)}, u32[]{:S(2)}) copy-start(bf16[512,256]{1,0:T(8,128)(2,1)} %param.16) | copy-start | bytes 786436
  107.3 171.1 %copy-start.5 = (bf16[256,256]{1,0:T(8,128)(2,1)S(1)}, bf16[256,256]{1,0:T(8,128)(2,1)}, u32[]{:S(2)}) copy-start(bf16[256,256]{1,0:T(8,128)(2,1)} %param.17) | copy-start | bytes 393220
  108.8 169.6 %all-gather.10.cloned.1.call-start = ((), (), s32[]{:S(2)}) async-start(), calls=%async_computation.6 | async-start | bytes 1179648 | tf_op jit(solution)/shard_map/all_gather | solution.py:43
  171.6 227.2 %all-gather.12.cloned.1.call-start = ((), (), s32[]{:S(2)}) async-start(), calls=%async_computation.7 | async-start | bytes 4718592 | tf_op jit(solution)/shard_map/all_gather | solution.py:56
  323.6 150.1 %all-gather.14.cloned.1.call-start = ((), (), s32[]{:S(2)}) async-start(), calls=%async_computation.8 | async-start | bytes 4718592 | tf_op jit(solution)/shard_map/all_gather | solution.py:57
Sparse Core Ops, SparseCore 0:
  10.1 42.9 all-gather.7
  55.3 47.7 all-gather.5
  107.1 62.6 reduce-scatter.4
  173.6 61.6 reduce-scatter.2
  237.9 40.5 all-gather.9
  323.7 75.0 all-gather.11
  400.9 72.8 all-gather.13
where the time goes:
time: 488 us; the launch traced here: 487 us
  waiting for transfers between devices  355 us (73%)
  blocking collectives  70.4 us (14%)
  local copies, waits for them, and re-layouts  21.8 us (4%)
  between operations  15.6 us (3%)
  matrix products  14.9 us (3%)
  other arithmetic  8.88 us (2%)
    all_gather x2, waiting for transfers between devices, projected_partial(): lax.all_gather(factor, 'fs', axis=0, tiled=True)  90.3 us
    all_gather x1, waiting for transfers between devices, on_device(): lax.all_gather(local_out, 'fs', axis=0, tiled=True)  68.5 us
    all_gather x1, waiting for transfers between devices, on_device(): lax.all_gather(local_gate, 'fs', axis=0, tiled=True)  64.3 us
    reduce_scatter x1, waiting for transfers between devices, on_device(): lax.psum_scatter(part_gate, 'fs', scatter_dimension=0, tiled=True)  62.3 us
    reduce_scatter x1, waiting for transfers between devices, on_device(): lax.psum_scatter(part_out, 'fs', scatter_dimension=0, tiled=True)  61 us
    psum x1, blocking collectives, on_device(): lax.psum((jnp.sum(update_gate * update_gate), jnp.sum(update_out * update...  38.7 us
    all_gather x1, blocking collectives, on_device(): lax.all_gather(normed_gate, 'fs', axis=0, tiled=True)  31.7 us
    unnamed x18, local copies, waits for them, and re-layouts  21.8 us
  transfers between devices with their start and end apart: 7, of which 7 were waited for; matrix products, arithmetic and copies ran while one was open for 7% of the time, Pallas kernels for 0%

commit v1 on v0

--- a/solution.py
+++ b/solution.py
@@ -45,7 +45,7 @@
     update_gate = jnp.dot(p_gate.astype(jnp.float32), whole_gate, precision=lax.Precision.HIGHEST)
     update_out = jnp.dot(p_out.astype(jnp.float32), whole_out, precision=lax.Precision.HIGHEST)
     squares = lax.psum(
-        (jnp.sum(update_gate * update_gate), jnp.sum(update_out * update_out)), ("fs", "tp")
+        lax.psum((jnp.sum(update_gate * update_gate), jnp.sum(update_out * update_out)), "tp"), "fs"
     )
     devices_all = lax.axis_size("fs") * lax.axis_size("tp")
     step_gate = update_gate * lax.rsqrt(squares[0] / (update_gate.size * devices_all) + EPSILON)

time: 488 us -> 472 us (0.967)
  blocking collectives: 70.4 us -> 57.9 us
    psum x1, blocking collectives: 38.7 us -> 6.27 us  [on_device(): lax.psum((jnp.sum(update_gate * update_gate), jnp.sum(update_out * update...]
    psum x0 -> x1, blocking collectives: none -> 19.9 us  [on_device(): lax.psum(lax.psum((jnp.sum(update_gate * update_gate), jnp.sum(update_out...]
where the time goes in v1:
time: 472 us; the launch traced here: 471 us
  waiting for transfers between devices  352 us (75%)
  blocking collectives  57.9 us (12%)
  local copies, waits for them, and re-layouts  21.8 us (5%)
  between operations  15.6 us (3%)
  matrix products  14.9 us (3%)
  other arithmetic  8.95 us (2%)
    all_gather x2, waiting for transfers between devices, projected_partial(): lax.all_gather(factor, 'fs', axis=0, tiled=True)  90.3 us
    all_gather x1, waiting for transfers between devices, on_device(): lax.all_gather(local_out, 'fs', axis=0, tiled=True)  68.5 us
    reduce_scatter x1, waiting for transfers between devices, on_device(): lax.psum_scatter(part_gate, 'fs', scatter_dimension=0, tiled=True)  62.3 us
    reduce_scatter x1, waiting for transfers between devices, on_device(): lax.psum_scatter(part_out, 'fs', scatter_dimension=0, tiled=True)  61 us
    all_gather x1, waiting for transfers between devices, on_device(): lax.all_gather(local_gate, 'fs', axis=0, tiled=True)  60.8 us
    all_gather x1, blocking collectives, on_device(): lax.all_gather(normed_gate, 'fs', axis=0, tiled=True)  31.7 us
    unnamed x18, local copies, waits for them, and re-layouts  21.8 us
    psum x1, blocking collectives, on_device(): lax.psum(lax.psum((jnp.sum(update_gate * update_gate), jnp.sum(update_out...  19.9 us
  transfers between devices with their start and end apart: 7, of which 7 were waited for; matrix products, arithmetic and copies ran while one was open for 7% of the time, Pallas kernels for 0%

profile of v1, /device:TPU:0, one launch (start us, length us, event | category | flops | bytes accessed | tf_op | source)
XLA Modules:
  0.0 471.1 jit_solution(8288790291037191959)
XLA Ops:
  8.7 44.4 %all-gather.8.cloned.1.call-done = bf16[2048,256]{1,0:T(8,128)(2,1)} async-done(((bf16[256,256]{1,0:T(8,128)(2,1)}), bf16[2048,256]{1,0:T(8,128)(2,1)}) %all-gather.8.cloned.1.call-update) | async-done | bytes 1048592 | tf_op jit(solution)/shard_map/all_gather | solution.py:15
  53.2 1.9 fusion.6
  55.1 2.0 fusion.7
  57.2 45.9 %all-gather.6.cloned.1.call-done = bf16[4096,256]{1,0:T(8,128)(2,1)} async-done(((bf16[512,256]{1,0:T(8,128)(2,1)}), bf16[4096,256]{1,0:T(8,128)(2,1)}) %all-gather.6.cloned.1.call-update) | async-done | bytes 2097168 | tf_op jit(solution)/shard_map/all_gather | solution.py:15
  103.1 4.2 fusion.4
  108.8 61.0 %reduce-scatter.5.cloned.1.call-done = f32[32,1024]{1,0:T(8,128)} async-done(((f32[256,1024]{1,0:T(8,128)}), f32[32,1024]{1,0:T(8,128)}) %reduce-scatter.5.cloned.1.call-update) | async-done | bytes 131088 | tf_op jit(solution)/shard_map/reduce_scatter | solution.py:33
  169.8 1.8 rsqrt_multiply_fusion
  173.0 62.3 %reduce-scatter.3.cloned.1.call-done = f32[32,512]{1,0:T(8,128)} async-done(((f32[256,512]{1,0:T(8,128)}), f32[32,512]{1,0:T(8,128)}) %reduce-scatter.3.cloned.1.call-update) | async-done | bytes 65552 | tf_op jit(solution)/shard_map/reduce_scatter | solution.py:32
  235.3 1.6 rsqrt_multiply_fusion.1
  236.9 31.7 %all_gather.19 = f32[256,512]{1,0:T(8,128)S(1)} all-gather(f32[32,512]{1,0:T(8,128)S(1)} %get-tuple-element.27), channel_id=1, replica_groups=mesh['fs'=8,'tp'=4] {'fs'}, dimensions={0}, use_global_device_ids=true | all-gather | bytes 589824 | tf_op jit(solution)/shard_map/all_gather | solution.py:42
  268.6 2.6 multiply_reduce_fusion.1
  271.1 7.3 %all-gather.10.cloned.1.call-done = f32[256,1024]{1,0:T(8,128)} async-done(((f32[32,1024]{1,0:T(8,128)}), f32[256,1024]{1,0:T(8,128)}) %all-gather.10.cloned.1.call-update) | async-done | bytes 1048592 | tf_op jit(solution)/shard_map/all_gather | solution.py:43
  278.4 2.8 multiply_reduce_fusion
  281.2 6.3 %all-reduce.1 = (f32[]{:T(128)}, f32[]{:T(128)}) all-reduce(f32[]{:T(128)} %get-tuple-element.30, f32[]{:T(128)} %get-tuple-element.32), channel_id=1, replica_groups=mesh['fs'=8,'tp'=4] {'tp'}, use_global_device_ids=true, to_apply=%region_2.0 | all-reduce | flops 2 | bytes 16 | tf_op jit(solution)/shard_map/psum | solution.py:48
  287.5 19.9 %all-reduce = (f32[]{:T(128)}, f32[]{:T(128)}) all-reduce(f32[]{:T(128)} %get-tuple-element.18, f32[]{:T(128)} %get-tuple-element.19), channel_id=1, replica_groups=mesh['fs'=8,'tp'=4] {'fs'}, use_global_device_ids=true, to_apply=%region_3.0 | all-reduce | flops 2 | bytes 16 | tf_op jit(solution)/shard_map/psum | solution.py:47
  308.1 2.9 subtract_convert_fusion.1
  311.2 2.5 copy.21
  314.4 2.6 subtract_convert_fusion
  317.0 2.6 copy.22
  319.6 2.5 copy.23
  322.1 60.8 %all-gather.12.cloned.1.call-done = bf16[4096,512]{0,1:T(8,128)(2,1)} async-done(((bf16[512,512]{0,1:T(8,128)(2,1)}), bf16[4096,512]{0,1:T(8,128)(2,1)}) %all-gather.12.cloned.1.call-update) | async-done | bytes 4194320 | tf_op jit(solution)/shard_map/all_gather | solution.py:56
  383.0 6.4 %copy.24 = bf16[4096,512]{1,0:T(8,128)(2,1)} copy(bf16[4096,512]{0,1:T(8,128)(2,1)} %all-gather.12.cloned.1.call-done) | data formatting | bytes 8388608
  389.4 68.5 %all-gather.14.cloned.1.call-done = bf16[2048,1024]{0,1:T(8,128)(2,1)} async-done(((bf16[256,1024]{0,1:T(8,128)(2,1)}), bf16[2048,1024]{0,1:T(8,128)(2,1)}) %all-gather.14.cloned.1.call-update) | async-done | bytes 4194320 | tf_op jit(solution)/shard_map/all_gather | solution.py:57
  457.9 6.4 %copy.25 = bf16[2048,1024]{1,0:T(8,128)(2,1)} copy(bf16[2048,1024]{0,1:T(8,128)(2,1)} %all-gather.14.cloned.1.call-done) | data formatting | bytes 8388608
  (28 shorter events, 4.5 us)
Async XLA Ops:
  7.2 46.0 %copy-start = (bf16[512,2048]{1,0:T(8,128)(2,1)S(1)}, bf16[512,2048]{1,0:T(8,128)(2,1)}, u32[]{:S(2)}) copy-start(bf16[512,2048]{1,0:T(8,128)(2,1)} %param.13) | copy-start | bytes 6291460
  7.2 47.9 %copy-start.1 = (bf16[512,1024]{1,0:T(8,128)(2,1)S(1)}, bf16[512,1024]{1,0:T(8,128)(2,1)}, u32[]{:S(2)}) copy-start(bf16[512,1024]{1,0:T(8,128)(2,1)} %param.15) | copy-start | bytes 3145732
  7.2 46.0 %all-gather.8.cloned.1.call-start = ((), (), s32[]{:S(2)}) async-start(), calls=%async_computation.4 | async-start | bytes 1179648 | tf_op jit(solution)/shard_map/all_gather | solution.py:15
  7.9 95.2 %all-gather.6.cloned.1.call-start = ((), (), s32[]{:S(2)}) async-start(), calls=%async_computation.2 | async-start | bytes 2359296 | tf_op jit(solution)/shard_map/all_gather | solution.py:15
  8.7 161.1 %reduce-scatter.5.cloned.1.call-start = ((), (), s32[]{:S(2)}) async-start(), calls=%async_computation.5 | async-start | bytes 1179648 | tf_op jit(solution)/shard_map/reduce_scatter | solution.py:33
  57.1 114.5 %copy-start.2 = (f32[512,512]{1,0:T(8,128)S(1)}, f32[512,512]{1,0:T(8,128)}, u32[]{:S(2)}) copy-start(f32[512,512]{1,0:T(8,128)} %param.18) | copy-start | bytes 3145732
  57.2 178.1 %reduce-scatter.3.cloned.1.call-start = ((), (), s32[]{:S(2)}) async-start(), calls=%async_computation.3 | async-start | bytes 589824 | tf_op jit(solution)/shard_map/reduce_scatter | solution.py:32
  103.1 4.2 copy-start.4
  107.3 161.3 %copy-start.3 = (bf16[512,256]{1,0:T(8,128)(2,1)S(1)}, bf16[512,256]{1,0:T(8,128)(2,1)}, u32[]{:S(2)}) copy-start(bf16[512,256]{1,0:T(8,128)(2,1)} %param.16) | copy-start | bytes 786436
  107.3 171.1 %copy-start.5 = (bf16[256,256]{1,0:T(8,128)(2,1)S(1)}, bf16[256,256]{1,0:T(8,128)(2,1)}, u32[]{:S(2)}) copy-start(bf16[256,256]{1,0:T(8,128)(2,1)} %param.17) | copy-start | bytes 393220
  108.8 169.6 %all-gather.10.cloned.1.call-start = ((), (), s32[]{:S(2)}) async-start(), calls=%async_computation.6 | async-start | bytes 1179648 | tf_op jit(solution)/shard_map/all_gather | solution.py:43
  171.6 211.4 %all-gather.12.cloned.1.call-start = ((), (), s32[]{:S(2)}) async-start(), calls=%async_computation.7 | async-start | bytes 4718592 | tf_op jit(solution)/shard_map/all_gather | solution.py:56
  311.1 146.8 %all-gather.14.cloned.1.call-start = ((), (), s32[]{:S(2)}) async-start(), calls=%async_computation.8 | async-start | bytes 4718592 | tf_op jit(solution)/shard_map/all_gather | solution.py:57
Sparse Core Ops, SparseCore 0:
  10.1 42.9 all-gather.7
  55.3 47.7 all-gather.5
  107.1 62.6 reduce-scatter.4
  173.6 61.6 reduce-scatter.2
  237.9 40.5 all-gather.9
  311.2 71.6 all-gather.11
  385.0 72.8 all-gather.13
